TPU v7x, 32 devices: a whole 2x2x4 slice. The times are simulated.
32 devices in a mesh: sp: 4 (over z), dp: 8 (over y, x, core).
Axes of the slice: x: 2, y: 2, z: 4, core: 2. Of those that a mesh axis runs over, the one named last changes fastest.
Arguments:
- cotangent: bfloat16 [8, 512, 2048], P('dp', 'sp'), may hold values from -6 to 6
- unit_pre: bfloat16 [8, 512, 2048], P('dp', None, 'sp'), may hold values from -6 to 6
- gate_pre: bfloat16 [8, 512, 2048], P('dp', None, 'sp'), may hold values from -15 to 15
- out_weight: bfloat16 [2048, 2048], P('dp', 'sp'), may hold values from -0.125 to 0.125
- mix_weight: bfloat16 [8, 128, 128], replicated, may hold values from -0.5 to 0.5
- mix_bias: bfloat16 [8, 128], replicated, may hold values from 0.099609375 to 1.8984375
- norm_gain: bfloat16 [2048], P('sp'), may hold values from 0.099609375 to 1.8984375
- norm_shift: bfloat16 [2048], P('sp'), may hold values from -3 to 3
Outputs:
- unit_grad: bfloat16 [8, 512, 2048], P('dp', None, 'sp')
- gate_grad: bfloat16 [8, 512, 2048], P('dp', None, 'sp')
- out_weight_grad: float32 [2048, 2048], P('dp', 'sp')
- mix_weight_grad: float32 [8, 128, 128], replicated
- mix_bias_grad: float32 [8, 128], replicated
- gain_grad: float32 [2048], P('sp')
- shift_grad: float32 [2048], P('sp')
All inputs are finite; a program needn't handle non-finite values.
Results may differ from a plain program's by a relative error of at most 0.015.
Values may be sent and summed in bfloat16 or wider, within the bound.
A program may use at most 64 MiB of HBM per device.

v0:
```python
import math

import jax
import jax.numpy as jnp
from jax import lax
from jax.sharding import PartitionSpec as P

GW = 2048
GROUPS = 8
BLK = 128


epsilon = 1e-05
tanh_coef = math.sqrt(2.0 / math.pi)


def gelu_slope(values):
    inner = tanh_coef * (values + 0.044715 * values * values * values)
    hyper = jnp.tanh(inner)
    return 0.5 * (1.0 + hyper) + 0.5 * values * (1.0 - hyper * hyper) * tanh_coef * (
        1.0 + 3.0 * 0.044715 * values * values
    )


def local(cotangent, unit_pre, gate_pre, out_weight, mix_weight, mix_bias, norm_gain, norm_shift):
    seq_len = unit_pre.shape[1]
    channels = unit_pre.shape[2]
    group_dim = GW // GROUPS
    span_width = min(channels, group_dim)
    groups_here = channels // span_width
    blocks = seq_len // BLK
    group_start = lax.axis_index("sp") * channels // group_dim
    units = unit_pre[0].astype(jnp.float32)
    gates = gate_pre[0].astype(jnp.float32)
    unit_act = jax.nn.gelu(units)
    gate_act = jax.nn.gelu(gates)
    moments = lax.psum((jnp.sum(gate_act, axis=-1), jnp.sum(gate_act * gate_act, axis=-1)), "sp")
    mean_val = moments[0] / GW
    var_val = moments[1] / GW - mean_val * mean_val
    rstd_val = lax.rsqrt(var_val + epsilon)
    centred = (gate_act - mean_val[:, None]) * rstd_val[:, None]
    gain_vec = norm_gain.astype(jnp.float32)
    normed = (centred * gain_vec + norm_shift.astype(jnp.float32)).astype(jnp.bfloat16)
    causal = jnp.arange(BLK)[:, None] >= jnp.arange(BLK)[None, :]
    local_weight = lax.dynamic_slice_in_dim(mix_weight, group_start, groups_here, 0)
    masked = jnp.where(causal[None], local_weight, jnp.zeros_like(local_weight))
    local_bias = lax.dynamic_slice_in_dim(mix_bias, group_start, groups_here, 0).astype(jnp.float32)
    normed_blocks = normed.reshape(blocks, BLK, groups_here, span_width)
    mixed = jnp.einsum("gts,nsgd->ntgd", masked, normed_blocks, preferred_element_type=jnp.float32)
    mixed = (mixed + local_bias.T[None, :, :, None]).reshape(seq_len, channels)
    gated = (unit_act * mixed).astype(jnp.bfloat16)
    weight_whole = lax.all_gather(out_weight, "dp", axis=0, tiled=True)
    dy_rows = lax.all_gather(cotangent, "sp", axis=1, tiled=True)[0]
    product = jnp.dot(dy_rows, weight_whole, preferred_element_type=jnp.float32)
    weight_part = lax.dot_general(
        dy_rows, gated, (((0,), (0,)), ((), ())), preferred_element_type=jnp.float32
    )
    token_count = lax.axis_size("dp") * seq_len
    norm_scale = 1.0 / math.sqrt(token_count)
    mix_scale = 1.0 / math.sqrt(token_count // BLK * group_dim)
    out_grad = (
        lax.psum_scatter(
            weight_part.astype(jnp.bfloat16), "dp", scatter_dimension=0, tiled=True
        ).astype(jnp.float32)
        * norm_scale
    )
    unit_grad = (product * mixed * gelu_slope(units)).astype(jnp.bfloat16)
    mix_grad = product * unit_act
    mix_round = mix_grad.astype(jnp.bfloat16).reshape(blocks, BLK, groups_here, span_width)
    mix_term = jnp.einsum(
        "ntgd,nsgd->gts", mix_round, normed_blocks, preferred_element_type=jnp.float32
    )
    mix_term = jnp.where(causal[None], mix_term, jnp.float32(0.0))
    bias_term = jnp.sum(mix_grad.reshape(blocks, BLK, groups_here, span_width), axis=(0, 3)).T
    normed_grad = jnp.einsum(
        "gts,ntgd->nsgd", masked, mix_round, preferred_element_type=jnp.float32
    ).reshape(seq_len, channels)
    gain_term = jnp.sum(normed_grad * centred, axis=0)
    shift_term = jnp.sum(normed_grad, axis=0)
    scaled = normed_grad * gain_vec
    back_sums = lax.psum((jnp.sum(scaled, axis=-1), jnp.sum(scaled * centred, axis=-1)), "sp")
    first_m = back_sums[0] / GW
    second_m = back_sums[1] / GW
    gate_grad = (
        rstd_val[:, None]
        * (scaled - first_m[:, None] - centred * second_m[:, None])
        * gelu_slope(gates)
    ).astype(jnp.bfloat16)
    empty_weight = jnp.zeros((GROUPS, BLK, BLK), jnp.float32)
    empty_bias = jnp.zeros((GROUPS, BLK), jnp.float32)
    mix_local, bias_local, gain_total, shift_total = (
        lax.psum(mix_term.astype(jnp.bfloat16), "dp").astype(jnp.float32),
        lax.psum(bias_term.astype(jnp.bfloat16), "dp").astype(jnp.float32),
        lax.psum(gain_term.astype(jnp.bfloat16), "dp").astype(jnp.float32),
        lax.psum(shift_term.astype(jnp.bfloat16), "dp").astype(jnp.float32),
    )
    full_weight = lax.dynamic_update_slice_in_dim(empty_weight, mix_local, group_start, 0)
    full_bias = lax.dynamic_update_slice_in_dim(empty_bias, bias_local, group_start, 0)
    full_weight, full_bias = (
        lax.psum(full_weight.astype(jnp.bfloat16), "sp").astype(jnp.float32),
        lax.psum(full_bias.astype(jnp.bfloat16), "sp").astype(jnp.float32),
    )
    return (
        unit_grad[None],
        gate_grad[None],
        out_grad,
        full_weight * mix_scale,
        full_bias * mix_scale,
        gain_total * norm_scale,
        shift_total * norm_scale,
    )


def solution(mesh):
    in_specs = (
        P("dp", "sp", None),
        P("dp", None, "sp"),
        P("dp", None, "sp"),
        P("dp", "sp"),
        P(),
        P(),
        P("sp"),
        P("sp"),
    )
    out_specs = (
        P("dp", None, "sp"),
        P("dp", None, "sp"),
        P("dp", "sp"),
        P(),
        P(),
        P("sp"),
        P("sp"),
    )
    return jax.shard_map(local, mesh=mesh, in_specs=in_specs, out_specs=out_specs, check_vma=False)
```

profile of v0, /device:TPU:0, one launch (start us, length us, event | category | flops | bytes accessed | tf_op | source)
XLA Modules:
  0.0 237.9 jit_solution(5552104702866696244)
XLA Ops:
  8.7 1.7 reshape.181
  11.7 1.3 copy.78
  13.5 13.9 %all-reduce.1 = (f32[512]{0:T(512)S(1)}, f32[512]{0:T(512)S(1)}) all-reduce(f32[512]{0:T(512)S(1)} %get-tuple-element.40, f32[512]{0:T(512)S(1)} %get-tuple-element.39), channel_id=1, replica_groups=mesh['sp'=4,'dp'=8] {'sp'}, use_global_device_ids=true, to_apply=%region_3.4 | all-reduce | flops 1024 | bytes 8192 | tf_op jit(solution)/shard_map/psum | solution.py:37
  28.2 3.3 %fusion.43 = (bf16[4,128,2,256]{1,3,0,2:T(8,128)(2,1)}, f32[4,128,2,256]{1,3,0,2:T(8,128)}) fusion(f32[4,128,2,256]{1,3,0,2:T(8,128)} %copy.78, f32[128,2]{0,1:T(2,128)S(1)} %convert_bitcast_fusion.1, bf16[8,128,128]{2,1,0:T(8,128)(2,1)S(1)} %copy-done.7, s32[]{:T(128)S(6)} %select_n.20, pred[128,128]{1,0:T(8,128)(4,1)S(1)} %iota_compare_fusion, ...), kind=kOutput, calls=%fused_computation.64 | convolution fusion | flops 73433088 | bytes 3761156 | tf_op jit(solution)/shard_map/gts,nsgd->ntgd/dot_general | solution.py:49
  31.5 1.5 copy.71
  33.0 1.0 copy.87
  34.1 24.0 %all-gather.3.cloned.1.call-done = bf16[1,512,2048]{2,1,0:T(8,128)(2,1)} async-done(((bf16[1,128,2048]{2,1,0:T(8,128)(2,1)}), bf16[1,512,2048]{2,1,0:T(8,128)(2,1)}) %all-gather.3.cloned.1.call-update) | async-done | bytes 2097168 | tf_op jit(solution)/shard_map/all_gather | solution.py:53
  58.0 28.5 %all-gather.5.cloned.1.call-done = bf16[2048,512]{1,0:T(8,128)(2,1)} async-done(((bf16[256,512]{1,0:T(8,128)(2,1)}), bf16[2048,512]{1,0:T(8,128)(2,1)}) %all-gather.5.cloned.1.call-update) | async-done | bytes 2097168 | tf_op jit(solution)/shard_map/all_gather | solution.py:52
  86.6 5.6 %fusion.85 = (bf16[512,512]{1,0:T(8,128)(2,1)}, f32[512,512]{1,0:T(8,128)S(1)}, bf16[1,512,512]{2,1,0:T(8,128)(2,1)}) fusion(bf16[1,512,512]{2,1,0:T(8,128)(2,1)S(1)} %copy-done.2, f32[512,512]{1,0:T(8,128)} %bitcast.107, bf16[2048,512]{1,0:T(8,128)(2,1)} %all-gather.5.cloned.1.call-done, bf16[1,512,2048]{2,1,0:T(8,128)(2,1)} %all-gather.3.cloned.1.call-done), kind=kOutput, calls=%fused_computation.126 | convolution fusion | flops 1081868288 | bytes 7864320 | tf_op jit(solution)/shard_map/dot_general | solution.py:54
  92.2 1.2 reshape.178
  93.3 1.4 fusion.10
  94.8 1.4 copy.79
  97.1 51.0 %all-reduce.6.cloned.1.call-done = bf16[2,128,128]{2,1,0:T(8,128)(2,1)} async-done(((bf16[2,128,128]{2,1,0:T(8,128)(2,1)}), bf16[2,128,128]{2,1,0:T(8,128)(2,1)}) %all-reduce.6.cloned.1.call-update) | async-done | bytes 65552 | tf_op jit(solution)/shard_map/psum | solution.py:92
  149.7 4.3 %fusion = bf16[2048,512]{0,1:T(8,128)(2,1)} fusion(bf16[512,512]{1,0:T(8,128)(2,1)} %bitcast.108, bf16[1,512,2048]{2,1,0:T(8,128)(2,1)} %all-gather.3.cloned.1.call-done), kind=kOutput, calls=%fused_computation.13 | convolution fusion | flops 1074790400 | bytes 4718592 | tf_op jit(solution)/shard_map/dot_general | solution.py:55
  154.1 1.0 copy-done.4
  155.1 1.8 multiply_reduce_fusion
  158.1 1.6 copy.73
  160.5 11.8 %all-reduce.2 = (bf16[2,128]{1,0:T(2,128)(2,1)S(1)}, bf16[512]{0:T(512)(128)(2,1)S(1)}, bf16[512]{0:T(512)(128)(2,1)S(1)}) all-reduce(bf16[2,128]{1,0:T(2,128)(2,1)S(1)} %bitcast.114, bf16[512]{0:T(512)(128)(2,1)S(1)} %bitcast.112, bf16[512]{0:T(512)(128)(2,1)S(1)} %bitcast.113), channel_id=1, replica_groups=mesh['sp'=4,'dp'=8] {'dp'}, use_global_device_ids=true, to_apply=%region_12.13 | all-reduce | flops 1280 | bytes 5120 | tf_op jit(solution)/shard_map/psum | solution.py:93
  172.4 12.0 %psum.77 = bf16[8,128]{1,0:T(8,128)(2,1)S(1)} all-reduce(bf16[8,128]{1,0:T(8,128)(2,1)S(1)} %dynamic_update_slice.7), channel_id=1, replica_groups=mesh['sp'=4,'dp'=8] {'sp'}, use_global_device_ids=true, to_apply=%region_13.14 | all-reduce | flops 1024 | bytes 4096 | tf_op jit(solution)/shard_map/psum | solution.py:101
  184.4 8.4 %all-reduce = (f32[512]{0:T(512)S(1)}, f32[512]{0:T(512)S(1)}) all-reduce(f32[512]{0:T(512)S(1)} %bitcast.115, f32[512]{0:T(512)S(1)} %bitcast.116), channel_id=1, replica_groups=mesh['sp'=4,'dp'=8] {'sp'}, use_global_device_ids=true, to_apply=%region_7.8 | all-reduce | flops 1024 | bytes 8192 | tf_op jit(solution)/shard_map/psum | solution.py:81
  193.9 2.1 fusion.69
  196.1 1.8 convert_multiply_fusion.9
  197.9 31.5 %reduce-scatter.2.cloned.1.call-done = bf16[256,512]{0,1:T(8,128)(2,1)} async-done(((bf16[2048,512]{0,1:T(8,128)(2,1)}), bf16[256,512]{0,1:T(8,128)(2,1)}) %reduce-scatter.2.cloned.1.call-update) | async-done | bytes 262160 | tf_op jit(solution)/shard_map/reduce_scatter | solution.py:62
  230.4 1.0 copy.83
  (50 shorter events, 10.8 us)
Async XLA Ops:
  7.2 50.9 %all-gather.3.cloned.1.call-start = ((), (), s32[]{:S(2)}) async-start(), calls=%async_computation.1 | async-start | bytes 2621440 | tf_op jit(solution)/shard_map/all_gather | solution.py:53
  7.9 3.0 %copy-start.5 = (bf16[512]{0:T(512)(128)(2,1)S(1)}, bf16[512]{0:T(512)(128)(2,1)}, u32[]{:S(2)}) copy-start(bf16[512]{0:T(512)(128)(2,1)} %param.14) | copy-start | bytes 3076
  7.9 3.1 %copy-start.6 = (bf16[512]{0:T(512)(128)(2,1)S(1)}, bf16[512]{0:T(512)(128)(2,1)}, u32[]{:S(2)}) copy-start(bf16[512]{0:T(512)(128)(2,1)} %param.15) | copy-start | bytes 3076
  7.9 3.1 %copy-start.2 = (bf16[1,512,512]{2,1,0:T(8,128)(2,1)S(1)}, bf16[1,512,512]{2,1,0:T(8,128)(2,1)}, u32[]{:S(2)}) copy-start(bf16[1,512,512]{2,1,0:T(8,128)(2,1)} %param.9) | copy-start | bytes 1572868
  7.9 78.7 %all-gather.5.cloned.1.call-start = ((), (), s32[]{:S(2)}) async-start(), calls=%async_computation.2 | async-start | bytes 2359296 | tf_op jit(solution)/shard_map/all_gather | solution.py:52
  8.7 139.4 %all-reduce.6.cloned.1.call-start = ((), (), s32[]{:S(2)}) async-start(), calls=%async_computation.4 | async-start | bytes 131072 | tf_op jit(solution)/shard_map/psum | solution.py:92
  11.0 2.0 copy-start
  11.0 17.2 %copy-start.7 = (bf16[8,128,128]{2,1,0:T(8,128)(2,1)S(1)}, bf16[8,128,128]{2,1,0:T(8,128)(2,1)}, u32[]{:S(2)}) copy-start(bf16[8,128,128]{2,1,0:T(8,128)(2,1)} %param.12) | copy-start | bytes 786436
  93.3 1.4 copy-start.3
  94.7 101.3 %all-reduce.8.cloned.1.call-start = ((), (), s32[]{:S(2)}) async-start(), calls=%async_computation.5 | async-start | bytes 524288 | tf_op jit(solution)/shard_map/psum | solution.py:100
  149.0 0.7 copy-start.1
  149.7 79.7 %reduce-scatter.2.cloned.1.call-start = ((), (), s32[]{:S(2)}) async-start(), calls=%async_computation.3 | async-start | bytes 2359296 | tf_op jit(solution)/shard_map/reduce_scatter | solution.py:62
  154.1 1.1 copy-start.4
Sparse Core Ops, SparseCore 0:
  9.5 48.4 all-gather.2
  59.9 26.6 all-gather.4
  94.9 53.1 all-reduce.5
  150.3 35.0 all-reduce.7
  188.4 40.9 reduce-scatter.1
where the time goes:
time: 238 us
  waiting for transfers between devices  136 us (57%)
  blocking collectives  46.1 us (19%)
  matrix products  16.3 us (7%)
  local copies, waits for them, and re-layouts  16.2 us (7%)
  between operations  14 us (6%)
  other arithmetic  8.61 us (4%)
    psum x1, waiting for transfers between devices, local(): lax.psum(mix_term.astype(jnp.bfloat16), 'dp').astype(jnp.float32)  51 us
    reduce_scatter x1, waiting for transfers between devices, local(): lax.psum_scatter(weight_part.astype(jnp.bfloat16), 'dp', scatter_dimensio...  31.5 us
    all_gather x1, waiting for transfers between devices, local(): weight_whole = lax.all_gather(out_weight, 'dp', axis=0, tiled=True)  28.5 us
    all_gather x1, waiting for transfers between devices, local(): dy_rows = lax.all_gather(cotangent, 'sp', axis=1, tiled=True)[0]  24 us
    psum x1, blocking collectives, local(): lax.psum((jnp.sum(gate_act, axis=-1), jnp.sum(gate_act * gate_act, axis=-...  13.9 us
    psum x1, blocking collectives, local(): lax.psum(full_bias.astype(jnp.bfloat16), 'sp').astype(jnp.float32)  12 us
    psum x1, blocking collectives, local(): lax.psum(bias_term.astype(jnp.bfloat16), 'dp').astype(jnp.float32)  11.8 us
    psum x1, blocking collectives, local(): lax.psum((jnp.sum(scaled, axis=-1), jnp.sum(scaled * centred, axis=-1)),...  8.36 us
  transfers between devices with their start and end apart: 5, of which 4 were waited for; matrix products, arithmetic and copies ran while one was open for 12% of the time, Pallas kernels for 0%

commit v1 on v0

v1 whole, which is shorter than its diff:
```python
import functools
import math

import jax
import jax.numpy as jnp
from jax import lax
from jax.experimental import pallas as pl
from jax.experimental.pallas import tpu as pltpu
from jax.sharding import PartitionSpec as P

epsilon = 1e-05
tanh_coef = math.sqrt(2.0 / math.pi)
f32 = jnp.float32
bf16 = jnp.bfloat16


def act_and_slope(x):
    square = x * x
    hyper = jnp.tanh(tanh_coef * (x + 0.044715 * square * x))
    half = 0.5 * (1.0 + hyper)
    slope = half + 0.5 * x * (1.0 - hyper * hyper) * tanh_coef * (1.0 + 3.0 * 0.044715 * square)
    return x * half, slope


def xor(value, k):
    bit, out = 0, value
    while (1 << bit) <= k:
        if (k >> bit) & 1:
            out = out + (1 - 2 * ((value // (1 << bit)) % 2)) * (1 << bit)
        bit += 1
    return out


def columns_to_rows(columns, height):
    lane = lax.broadcasted_iota(jnp.int32, (height, 128), 1)
    wide = jnp.zeros((height, 128), f32)
    for i, column in enumerate(columns):
        wide = jnp.where(lane == i, column, wide)
    return jnp.transpose(wide)[0:8]


def rows_to_columns(rows):
    tall = jnp.concatenate([rows, jnp.zeros((120, rows.shape[1]), f32)], axis=0)
    return jnp.transpose(tall)


def kernel(
    n, m, width, group_dim, norm_scale, mix_scale,
    cot, unit, gate, w, mixw, mixb, gain, shift,
    unit_out, gate_out, w_out, mix_out, small_out,
    dyg, wg, cen, gsl, uact, uslope, mixed, normed, gatedt, scaled, acc,
    masked, maskedt, bcol, mixacc, biasacc, vecacc,
    mst, mrv, bst, brv, vst, vrv, vag, mbuf, mrecv, mout,
    part, precv, big, bigrecv,
    ring_s, ring_r, wd_s, wd_r, wf_s, wf_r, m_s, m_r, b_s, b_r, v_s, v_r,
    va_s, va_r, x_s, x_r, xa_s, xa_r, xo_s, xo_r, p_s, p_r, g_s, g_r, loc,
):
    ch = unit.shape[1]
    blk = mixw.shape[1]
    span = min(ch, group_dim)
    gh = ch // span
    dm = w_out.shape[0]
    half = n // 2
    hm = m // 2
    rows = mbuf.shape[1]
    sp = lax.axis_index("sp")
    dp = lax.axis_index("dp")
    core = dp % 2
    pair = dp // 2

    def remote(src, dst, s, r, **where):
        return pltpu.make_async_remote_copy(
            src_ref=src, dst_ref=dst, send_sem=s, recv_sem=r,
            device_id=where, device_id_type=pl.DeviceIdType.MESH,
        )

    def peer_sp(k):
        return (sp + k) % n

    load_c = pltpu.make_async_copy(cot, dyg.at[sp], loc.at[0])
    load_w = pltpu.make_async_copy(w, wg.at[dp], loc.at[1])
    load_c.start()
    load_w.start()
    barrier = pltpu.get_barrier_semaphore()
    for k in range(1, n):
        pl.semaphore_signal(barrier, inc=1, device_id={"sp": peer_sp(k)}, device_id_type=pl.DeviceIdType.MESH)
    for k in range(1, m):
        pl.semaphore_signal(barrier, inc=1, device_id={"dp": xor(dp, k)}, device_id_type=pl.DeviceIdType.MESH)

    def stats(b, carry):
        rs = pl.ds(pl.multiple_of(b * blk, blk), blk)
        value, slope = act_and_slope(gate[rs, :].astype(f32))
        cen[b] = value
        gsl[b] = slope
        mst[b] = columns_to_rows(
            [jnp.sum(value, axis=1, keepdims=True), jnp.sum(value * value, axis=1, keepdims=True)], blk
        )
        return carry

    lax.fori_loop(0, n, stats, 0)
    pl.semaphore_wait(barrier, n + m - 2)
    load_w.wait()

    wd = {
        k: remote(wg.at[dp], wg.at[dp], wd_s.at[k], wd_r.at[k], dp=2 * xor(pair, k) + core)
        for k in range(1, hm)
    }
    for k in reversed(range(1, hm)):
        wd[k].start()
    wf = [
        remote(wg.at[2 * xor(pair, k) + core], wg.at[2 * xor(pair, k) + core],
               wf_s.at[k], wf_r.at[k], dp=xor(dp, 1))
        for k in range(hm)
    ]
    wf[0].start()
    mo = {k: remote(mst, mrv.at[k], m_s.at[k], m_r.at[k], sp=peer_sp(k)) for k in range(1, n)}
    for k in range(1, n):
        mo[k].start()
    load_c.wait()

    def ring(step, direction, full):
        sign = 1 - 2 * direction
        owner = (sp - sign * (step - 1) + 2 * n) % n
        ref = dyg.at[owner]
        if not full:
            cut = blk // 2
            ref = dyg.at[owner, pl.ds(direction * cut, cut)]
        return remote(ref, ref, ring_s.at[direction, step], ring_r.at[direction, step], sp=(sp + sign + n) % n)

    def ring_start(step, full):
        ring(step, 0, full).start()
        ring(step, 1, full).start()

    def ring_recv(step, full):
        ring(step, 0, full).wait_recv()
        ring(step, 1, full).wait_recv()

    ring_start(1, half > 1)

    def units(b, carry):
        rs = pl.ds(pl.multiple_of(b * blk, blk), blk)
        uact[b], uslope[b] = act_and_slope(unit[rs, :].astype(f32))
        return carry

    lax.fori_loop(0, n, units, 0)

    causal = lax.broadcasted_iota(jnp.int32, (blk, blk), 0) >= lax.broadcasted_iota(jnp.int32, (blk, blk), 1)
    lane = lax.broadcasted_iota(jnp.int32, (blk, 128), 1)
    bias_t = rows_to_columns(mixb[...].astype(f32))
    start = sp * ch // group_dim
    for g in range(gh):
        one = jnp.where(causal, mixw[start + g].astype(f32), 0.0)
        masked[g] = one.astype(bf16)
        maskedt[g] = jnp.transpose(one).astype(bf16)
        bcol[g] = jnp.broadcast_to(
            jnp.sum(jnp.where(lane == start + g, bias_t, 0.0), axis=1, keepdims=True), (blk, 128)
        )
    gain_row = gain[...].astype(f32)
    shift_row = shift[...].astype(f32)
    for k in range(1, n):
        mo[k].wait_recv()

    def forward(b, carry):
        total = mst[b]
        for k in range(1, n):
            total = total + mrv[k, b]
        cols = rows_to_columns(total)
        mean = cols[:, 0:1] / width
        var = cols[:, 1:2] / width - mean * mean
        rstd = lax.rsqrt(var + epsilon)
        centred = (cen[b] - mean) * rstd
        cen[b] = centred
        gsl[b] = gsl[b] * rstd
        nb = (centred * gain_row + shift_row).astype(bf16)
        normed[b] = nb
        for g in range(gh):
            cs = slice(g * span, (g + 1) * span)
            mixg = jnp.dot(masked[g], nb[:, cs], preferred_element_type=f32) + bcol[g][:, 0:1]
            mixed[b, :, cs] = mixg
            gatedt[b, cs, :] = jnp.transpose(uact[b, :, cs] * mixg).astype(bf16)
        return carry

    lax.fori_loop(0, n, forward, 0)
    mixacc[...] = jnp.zeros_like(mixacc)
    biasacc[...] = jnp.zeros_like(biasacc)
    vecacc[...] = jnp.zeros_like(vecacc)

    ring_recv(1, half > 1)
    if half > 1:
        ring_start(2, half > 2)
    for k in reversed(range(1, hm)):
        wd[k].wait_recv()
        wf[k].start()
    for k in range(hm):
        wf[k].wait_recv()

    def block(o):
        rs = pl.ds(pl.multiple_of(o * blk, blk), blk)
        whole = wg[...].reshape(m * dm, ch)
        head = jnp.dot(dyg[o], whole, preferred_element_type=f32)
        unit_out[rs, :] = (head * mixed[o] * uslope[o]).astype(bf16)
        grad = head * uact[o]
        biasacc[...] += grad
        rounded = grad.astype(bf16)
        first = jnp.zeros((blk, 1), f32)
        second = jnp.zeros((blk, 1), f32)
        for g in range(gh):
            cs = slice(g * span, (g + 1) * span)
            mixacc[g] += lax.dot_general(
                rounded[:, cs], normed[o, :, cs], (((1,), (1,)), ((), ())), preferred_element_type=f32
            )
            ng = jnp.dot(maskedt[g], rounded[:, cs], preferred_element_type=f32)
            centred = cen[o, :, cs]
            vecacc[0:1, cs] += jnp.sum(ng * centred, axis=0, keepdims=True)
            vecacc[1:2, cs] += jnp.sum(ng, axis=0, keepdims=True)
            sc = ng * gain_row[:, cs]
            scaled[o, :, cs] = sc
            first = first + jnp.sum(sc, axis=1, keepdims=True)
            second = second + jnp.sum(sc * centred, axis=1, keepdims=True)
        bst[o] = columns_to_rows([first, second], blk)

    def weight(o, k):
        return jnp.dot(gatedt[o], dyg[o, :, k * dm:(k + 1) * dm], preferred_element_type=f32)

    def weights(o):
        for k in range(m):
            acc[k] += weight(o, k)

    block(sp)
    for k in range(m):
        acc[k] = weight(sp, k)

    def middle(step):
        def one(side, carry):
            o = (sp + (2 * side - 1) * step + n) % n
            block(o)
            weights(o)
            return carry

        lax.fori_loop(0, 2, one, 0)

    for step in range(1, half):
        if step > 1:
            ring_recv(step, True)
            ring_start(step + 1, step + 1 < half)
        middle(step)
    if half > 1:
        ring_recv(half, False)
    last = (sp + half) % n
    block(last)

    for g in range(gh):
        one = jnp.where(causal, mixacc[g], 0.0).astype(bf16)
        per = blk // rows
        for i in range(per):
            mbuf[g * per + i] = one[i * rows:(i + 1) * rows]
    bias_rows = columns_to_rows(
        [jnp.sum(biasacc[:, g * span:(g + 1) * span], axis=1, keepdims=True) for g in range(gh)], blk
    )
    vst[0:2, :] = vecacc[0:2, :]
    vst[2:2 + gh, 0:blk] = bias_rows[0:gh]
    xo = {k: remote(mbuf.at[xor(dp, k)], mrecv.at[k], x_s.at[k], x_r.at[k], dp=xor(dp, k)) for k in range(1, m)}
    vo = {k: remote(vst, vrv.at[k], v_s.at[k], v_r.at[k], dp=xor(dp, k)) for k in range(1, m)}
    bo = {k: remote(bst, brv.at[k], b_s.at[k], b_r.at[k], sp=peer_sp(k)) for k in range(1, n)}
    for k in reversed(range(1, m)):
        xo[k].start()
    for k in reversed(range(1, m)):
        vo[k].start()
    for k in range(1, n):
        bo[k].start()

    for k in range(m):
        acc[k] += weight(last, k)
    po = {}
    for k in reversed(range(hm)):
        other = 2 * xor(pair, k) + 1 - core
        part[k] = acc[other].astype(bf16)
        po[k] = remote(part.at[k], precv.at[k], p_s.at[k], p_r.at[k], dp=xor(dp, 1))
        po[k].start()

    for k in range(1, m):
        xo[k].wait_recv()
    total = mbuf[dp].astype(f32)
    for k in range(1, m):
        total = total + mrecv[k].astype(f32)
    mout[sp, dp] = total.astype(bf16)
    xa = {
        k: remote(mout.at[sp, dp], mout.at[sp, dp], xa_s.at[k], xa_r.at[k], dp=xor(dp, k)) for k in range(1, m)
    }
    for k in reversed(range(1, m)):
        xa[k].start()

    go = {}
    for k in reversed(range(1, hm)):
        po[k].wait_recv()
        big[k] = (acc[2 * xor(pair, k) + core] + precv[k].astype(f32)).astype(bf16)
        go[k] = remote(big.at[k], bigrecv.at[k], g_s.at[k], g_r.at[k], dp=2 * xor(pair, k) + core)
        go[k].start()
    po[0].wait_recv()

    for k in range(1, m):
        vo[k].wait_recv()
    vec = vst[...]
    for k in range(1, m):
        vec = vec + vrv[k]
    vag[sp] = vec
    va = {k: remote(vag.at[sp], vag.at[sp], va_s.at[k], va_r.at[k], sp=peer_sp(k)) for k in range(1, n)}
    for k in range(1, n):
        va[k].start()
    for k in range(1, m):
        xa[k].wait_recv()
    xs = {k: remote(mout.at[sp], mout.at[sp], xo_s.at[k], xo_r.at[k], sp=peer_sp(k)) for k in range(1, n)}
    for k in range(1, n):
        xs[k].start()

    for k in range(1, n):
        bo[k].wait_recv()

    def finish(b, carry):
        rs = pl.ds(pl.multiple_of(b * blk, blk), blk)
        total = bst[b]
        for k in range(1, n):
            total = total + brv[k, b]
        cols = rows_to_columns(total)
        gate_out[rs, :] = (
            gsl[b] * (scaled[b] - cols[:, 0:1] / width - cen[b] * (cols[:, 1:2] / width))
        ).astype(bf16)
        return carry

    lax.fori_loop(0, n, finish, 0)
    for k in range(1, n):
        va[k].wait_recv()
    small_out[...] = vag[...]
    for k in range(1, n):
        xs[k].wait_recv()
    mix_out[...] = mout[...].astype(f32) * mix_scale

    own = acc[dp] + precv[0].astype(f32)
    for k in range(1, hm):
        go[k].wait_recv()
        own = own + bigrecv[k].astype(f32)
    w_out[...] = jnp.transpose(own * norm_scale)

    for step in range(1, half + 1):
        ring(step, 0, step < half).wait_send()
        ring(step, 1, step < half).wait_send()
    sent = list(wd.values()) + wf + list(po.values())
    for group in (mo, xo, vo, bo, xa, go, va, xs):
        sent += list(group.values())
    for copy in sent:
        copy.wait_send()


def local(cotangent, unit_pre, gate_pre, out_weight, mix_weight, mix_bias, norm_gain, norm_shift):
    n, m = lax.axis_size("sp"), lax.axis_size("dp")
    groups, blk = mix_bias.shape
    seq, ch = unit_pre.shape[1:]
    width = ch * n
    dm, d = out_weight.shape[0], cotangent.shape[2]
    group_dim = width // groups
    span = min(ch, group_dim)
    gh = ch // span
    assert cotangent.shape[1] == blk and n % 2 == 0 and m & (m - 1) == 0
    rows = gh * blk // m
    hm = m // 2
    tokens = m * seq
    norm_scale = 1.0 / math.sqrt(tokens)
    mix_scale = 1.0 / math.sqrt(tokens // blk * group_dim)
    vm = pl.BlockSpec(memory_space=pltpu.VMEM)
    hbm = pl.BlockSpec(memory_space=pl.ANY)
    V = pltpu.VMEM
    dma = pltpu.SemaphoreType.DMA
    scratch = [
        V((n, blk, d), bf16), V((m, dm, ch), bf16),
        V((n, blk, ch), f32), V((n, blk, ch), f32), V((n, blk, ch), f32), V((n, blk, ch), f32),
        V((n, blk, ch), f32), V((n, blk, ch), bf16), V((n, ch, blk), bf16), V((n, blk, ch), f32),
        V((m, ch, dm), f32),
        V((gh, blk, blk), bf16), V((gh, blk, blk), bf16), V((gh, blk, 128), f32),
        V((gh, blk, blk), f32), V((blk, ch), f32), V((8, ch), f32),
        V((n, 8, blk), f32), V((n, n, 8, blk), f32), V((n, 8, blk), f32), V((n, n, 8, blk), f32),
        V((8, ch), f32), V((m, 8, ch), f32), V((n, 8, ch), f32),
        V((m, rows, blk), bf16), V((m, rows, blk), bf16), V((n, m, rows, blk), bf16),
        V((hm, ch, dm), bf16), V((hm, ch, dm), bf16), V((hm, ch, dm), bf16), V((hm, ch, dm), bf16),
        dma((2, n)), dma((2, n)),
        dma((hm,)), dma((hm,)), dma((hm,)), dma((hm,)),
        dma((n,)), dma((n,)), dma((n,)), dma((n,)), dma((m,)), dma((m,)),
        dma((n,)), dma((n,)), dma((m,)), dma((m,)), dma((m,)), dma((m,)), dma((n,)), dma((n,)),
        dma((hm,)), dma((hm,)), dma((hm,)), dma((hm,)), dma((2,)),
    ]
    unit_grad, gate_grad, w_grad, mix, small = pl.pallas_call(
        functools.partial(kernel, n, m, width, group_dim, norm_scale, mix_scale),
        out_shape=(
            jax.ShapeDtypeStruct((seq, ch), bf16),
            jax.ShapeDtypeStruct((seq, ch), bf16),
            jax.ShapeDtypeStruct((dm, ch), f32),
            jax.ShapeDtypeStruct((n, m, rows, blk), f32),
            jax.ShapeDtypeStruct((n, 8, ch), f32),
        ),
        in_specs=[hbm, vm, vm, hbm, vm, vm, vm, vm],
        out_specs=(vm,) * 5,
        scratch_shapes=scratch,
        compiler_params=pltpu.CompilerParams(
            collective_id=0, has_side_effects=True, vmem_limit_bytes=60 * 1024 * 1024
        ),
    )(
        cotangent[0], unit_pre[0], gate_pre[0], out_weight, mix_weight, mix_bias,
        norm_gain[None], norm_shift[None],
    )
    share = group_dim // span
    mix = jnp.sum(mix.reshape(groups, share, blk, blk), axis=1)
    bias = jnp.sum(small[:, 2:2 + gh, :blk].reshape(groups, share, blk), axis=1) * mix_scale
    mine = lax.dynamic_index_in_dim(small, lax.axis_index("sp"), 0, keepdims=False)
    return (
        unit_grad[None], gate_grad[None], w_grad, mix, bias, mine[0] * norm_scale, mine[1] * norm_scale,
    )


def solution(mesh):
    in_specs = (
        P("dp", "sp", None),
        P("dp", None, "sp"),
        P("dp", None, "sp"),
        P("dp", "sp"),
        P(),
        P(),
        P("sp"),
        P("sp"),
    )
    out_specs = (
        P("dp", None, "sp"),
        P("dp", None, "sp"),
        P("dp", "sp"),
        P(),
        P(),
        P("sp"),
        P("sp"),
    )
    return jax.shard_map(local, mesh=mesh, in_specs=in_specs, out_specs=out_specs, check_vma=False)
```

time: 238 us -> 76.2 us (0.32)
  waiting for transfers between devices: 136 us -> 0 us
  Pallas kernels: 0 us -> 65.3 us
  blocking collectives: 46.1 us -> 0 us
  matrix products: 16.3 us -> 0 us
  between operations: 14 us -> 0.66 us
  local copies, waits for them, and re-layouts: 16.2 us -> 7.11 us
  other arithmetic: 8.61 us -> 2.7 us
    pallas_call x0 -> x1, Pallas kernels: none -> 65.3 us  [local(): pl.pallas_call(functools.partial(kernel, n, m, width, group_dim, norm_sca...]
    all_gather x2 -> x0, waiting for transfers between devices: 52.5 us -> none  [the longest x1 28.5 us: local(): weight_whole = lax.all_gather(out_weight, 'dp', axis=0, tiled=True)]
    psum x2 -> x0, waiting for transfers between devices: 51 us -> none  [the longest x1 51 us: local(): lax.psum(mix_term.astype(jnp.bfloat16), 'dp').astype(jnp.float32)]
    psum x4 -> x0, blocking collectives: 46.1 us -> none  [the longest x1 13.9 us: local(): lax.psum((jnp.sum(gate_act, axis=-1), jnp.sum(gate_act * gate_act, axis=-...]
    reduce_scatter x1 -> x0, waiting for transfers between devices: 31.5 us -> none  [local(): lax.psum_scatter(weight_part.astype(jnp.bfloat16), 'dp', scatter_dimensio...]
    dot_general x5 -> x0, matrix products: 16.3 us -> none  [the longest x1 5.57 us: local(): product = jnp.dot(dy_rows, weight_whole, preferred_element_type=jnp.float32)]
    convert_element_type x5 -> x0, local copies, waits for them, and re-layouts: 5.51 us -> none  [the longest x2 2.19 us: local(): gates = gate_pre[0].astype(jnp.float32)]
    reshape x3 -> x0, local copies, waits for them, and re-layouts: 2.68 us -> none  [the longest x1 1.16 us: local(): mix_grad.astype(jnp.bfloat16).reshape(blocks, BLK, groups_here, span_width)]
  transfers between devices with their start and end apart: 5 -> 0, of which waited for: 4 -> 0; matrix products, arithmetic and copies ran while one was open for 12% -> 0% of each run, Pallas kernels for 0% -> 0%
where the time goes in v1:
time: 76.2 us; the launch traced here: 75.8 us
  Pallas kernels  65.3 us (86%)
  local copies, waits for them, and re-layouts  7.11 us (9%)
  other arithmetic  2.7 us (4%)
    pallas_call x1, Pallas kernels, local(): pl.pallas_call(functools.partial(kernel, n, m, width, group_dim, norm_sca...  65.3 us
    unnamed x14, local copies, waits for them, and re-layouts  5.95 us

profile of v1, /device:TPU:0, one launch (start us, length us, event | category | flops | bytes accessed | tf_op | source)
XLA Modules:
  0.0 75.8 jit_solution(8980352169402614919)
XLA Ops:
  0.6 0.0 copy-start.3
  0.6 0.7 copy-done.3
  1.3 0.0 copy-start.4
  1.3 0.6 broadcast_in_dim.12.gain
  1.9 0.1 copy-done.4
  2.0 0.6 broadcast_in_dim.13.shift
  2.6 65.3 %shard_map.135 = (bf16[512,512]{1,0:T(8,128)(2,1)}, bf16[512,512]{1,0:T(8,128)(2,1)}, f32[256,512]{1,0:T(8,128)}, f32[4,8,32,128]{3,2,1,0:T(8,128)}, f32[4,8,512]{2,1,0:T(8,128)}) custom-call(bf16[128,2048]{1,0:T(8,128)(2,1)} %bitcast.9, bf16[512,512]{1,0:T(8,128)(2,1)} %bitcast.10, bf16[512,512]{1,0:T(8,128)(2,1)} %bitcast.11, bf16[256,512]{1,0:T(8,128)(2,1)} %w.1, ...), custom_call_target="tpu_custom_call" | custom-call | tf_op jit(solution)/shard_map/pallas_call | solution.py:390
  67.9 1.4 %dynamic-slice_multiply_fusion = (f32[1,1,512]{2,1,0:T(1,128)}, f32[1,1,512]{2,1,0:T(1,128)}) fusion(f32[4,8,512]{2,1,0:T(8,128)} %get-tuple-element.16, s32[]{:T(128)S(6)} %select_n.4, s32[]{:T(128)S(6)} %add.5), kind=kLoop, calls=%fused_computation.1 | loop fusion | flops 1024 | bytes 8200 | tf_op jit(solution)/shard_map/mul | solution.py:414
  69.3 1.3 %slice_multiply_fusion = f32[4,2,128]{2,1,0:T(2,128)} fusion(f32[4,8,512]{2,1,0:T(8,128)} %get-tuple-element.16), kind=kLoop, calls=%fused_computation | loop fusion | flops 1024 | bytes 8192 | tf_op jit(solution)/shard_map/mul | solution.py:411
  70.6 0.0 copy-start.2
  70.6 1.9 %copy.19 = bf16[1,512,512]{2,1,0:T(8,128)(2,1)} copy(bf16[1,512,512]{2,1,0:T(8,128)(2,1)} %bitcast.14) | data formatting | bytes 1048576
  72.6 0.0 copy-done.2
  72.6 0.0 copy-start.1
  72.6 0.8 %copy.20 = bf16[1,512,512]{2,1,0:T(8,128)(2,1)} copy(bf16[1,512,512]{2,1,0:T(8,128)(2,1)S(1)} %bitcast.13) | data formatting | bytes 1048576
  73.4 0.4 copy-done.1
  73.8 0.0 copy-start
  73.8 0.8 %copy.21 = f32[256,512]{1,0:T(8,128)} copy(f32[256,512]{1,0:T(8,128)S(1)} %copy-done.1) | data formatting | bytes 1048576
  74.6 0.4 copy-done
  75.0 0.8 %copy.22 = f32[8,128,128]{2,1,0:T(8,128)} copy(f32[8,128,128]{2,1,0:T(8,128)S(1)} %bitcast.12) | data formatting | bytes 1048576
Async XLA Ops:
  0.6 0.7 copy-start.3
  1.3 0.7 copy-start.4
  70.6 1.9 %copy-start.2 = (bf16[512,512]{1,0:T(8,128)(2,1)S(1)}, bf16[512,512]{1,0:T(8,128)(2,1)}, u32[]{:S(2)}) copy-start(bf16[512,512]{1,0:T(8,128)(2,1)} %get-tuple-element.13) | copy-start | bytes 1572868
  72.6 1.2 %copy-start.1 = (f32[256,512]{1,0:T(8,128)S(1)}, f32[256,512]{1,0:T(8,128)}, u32[]{:S(2)}) copy-start(f32[256,512]{1,0:T(8,128)} %get-tuple-element.28) | copy-start | bytes 1572868
  73.8 1.2 %copy-start = (f32[4,8,32,128]{3,2,1,0:T(8,128)S(1)}, f32[4,8,32,128]{3,2,1,0:T(8,128)}, u32[]{:S(2)}) copy-start(f32[4,8,32,128]{3,2,1,0:T(8,128)} %get-tuple-element.15) | copy-start | bytes 1572868

commit v2 on v1

--- a/solution.py
+++ b/solution.py
@@ -53,7 +53,7 @@
     mst, mrv, bst, brv, vst, vrv, vag, mbuf, mrecv, mout,
     part, precv, big, bigrecv,
     ring_s, ring_r, wd_s, wd_r, wf_s, wf_r, m_s, m_r, b_s, b_r, v_s, v_r,
-    va_s, va_r, x_s, x_r, xa_s, xa_r, xo_s, xo_r, p_s, p_r, g_s, g_r, loc,
+    va_s, va_r, x_s, x_r, xa_s, xa_r, xo_s, xo_r, xf_s, xf_r, p_s, p_r, g_s, g_r, loc,
 ):
     ch = unit.shape[1]
     blk = mixw.shape[1]
@@ -118,24 +118,30 @@
         mo[k].start()
     load_c.wait()
 
-    def ring(step, direction, full):
+    def ring(step, direction, piece):
         sign = 1 - 2 * direction
         owner = (sp - sign * (step - 1) + 2 * n) % n
-        ref = dyg.at[owner]
-        if not full:
-            cut = blk // 2
-            ref = dyg.at[owner, pl.ds(direction * cut, cut)]
-        return remote(ref, ref, ring_s.at[direction, step], ring_r.at[direction, step], sp=(sp + sign + n) % n)
-
-    def ring_start(step, full):
-        ring(step, 0, full).start()
-        ring(step, 1, full).start()
-
-    def ring_recv(step, full):
-        ring(step, 0, full).wait_recv()
-        ring(step, 1, full).wait_recv()
-
-    ring_start(1, half > 1)
+        cut = blk // 2
+        ref = dyg.at[owner, pl.ds((direction + piece) % 2 * cut, cut)]
+        lane = 2 * direction + piece
+        return remote(ref, ref, ring_s.at[lane, step], ring_r.at[lane, step], sp=(sp + sign + n) % n)
+
+    def ring_start(step, piece):
+        ring(step, 0, piece).start()
+        ring(step, 1, piece).start()
+
+    def ring_recv(step, piece):
+        ring(step, 0, piece).wait_recv()
+        ring(step, 1, piece).wait_recv()
+
+    def ring_pass(step, piece):
+        ring_recv(step, piece)
+        if piece == 0 or step + 1 < half:
+            ring_start(step + 1, piece)
+
+    ring_start(1, 0)
+    if half > 1:
+        ring_start(1, 1)
 
     def units(b, carry):
         rs = pl.ds(pl.multiple_of(b * blk, blk), blk)
@@ -181,13 +187,12 @@
         return carry
 
     lax.fori_loop(0, n, forward, 0)
+    if half > 1:
+        ring_pass(1, 0)
     mixacc[...] = jnp.zeros_like(mixacc)
     biasacc[...] = jnp.zeros_like(biasacc)
     vecacc[...] = jnp.zeros_like(vecacc)
 
-    ring_recv(1, half > 1)
-    if half > 1:
-        ring_start(2, half > 2)
     for k in reversed(range(1, hm)):
         wd[k].wait_recv()
         wf[k].start()
@@ -241,11 +246,10 @@
 
     for step in range(1, half):
         if step > 1:
-            ring_recv(step, True)
-            ring_start(step + 1, step + 1 < half)
+            ring_pass(step, 0)
+        ring_pass(step, 1)
         middle(step)
-    if half > 1:
-        ring_recv(half, False)
+    ring_recv(half, 0)
     last = (sp + half) % n
     block(last)
 
@@ -309,7 +313,16 @@
         va[k].start()
     for k in range(1, m):
         xa[k].wait_recv()
-    xs = {k: remote(mout.at[sp], mout.at[sp], xo_s.at[k], xo_r.at[k], sp=peer_sp(k)) for k in range(1, n)}
+    share = pl.ds(core * hm, hm)
+    xs = {
+        k: remote(mout.at[sp, share], mout.at[sp, share], xo_s.at[k], xo_r.at[k], sp=peer_sp(k))
+        for k in range(1, n)
+    }
+    xf = {
+        k: remote(mout.at[(sp - k + n) % n, share], mout.at[(sp - k + n) % n, share],
+                  xf_s.at[k], xf_r.at[k], dp=xor(dp, 1))
+        for k in range(1, n)
+    }
     for k in range(1, n):
         xs[k].start()
 
@@ -333,6 +346,9 @@
     small_out[...] = vag[...]
     for k in range(1, n):
         xs[k].wait_recv()
+        xf[k].start()
+    for k in range(1, n):
+        xf[k].wait_recv()
     mix_out[...] = mout[...].astype(f32) * mix_scale
 
     own = acc[dp] + precv[0].astype(f32)
@@ -342,13 +358,42 @@
     w_out[...] = jnp.transpose(own * norm_scale)
 
     for step in range(1, half + 1):
-        ring(step, 0, step < half).wait_send()
-        ring(step, 1, step < half).wait_send()
+        for piece in range(2 if step < half else 1):
+            ring(step, 0, piece).wait_send()
+            ring(step, 1, piece).wait_send()
     sent = list(wd.values()) + wf + list(po.values())
-    for group in (mo, xo, vo, bo, xa, go, va, xs):
+    for group in (mo, xo, vo, bo, xa, go, va, xs, xf):
         sent += list(group.values())
     for copy in sent:
         copy.wait_send()
+
+
+def finish_kernel(
+    share, mix_scale, norm_scale, unit_in, gate_in, w_in, mix_in, small_in,
+    unit_out, gate_out, w_out, mix_out, bias_out, gain_out, shift_out, sems,
+):
+    copies = [
+        pltpu.make_async_copy(src, dst, sems.at[i])
+        for i, (src, dst) in enumerate(
+            ((unit_in, unit_out.at[0]), (gate_in, gate_out.at[0]), (w_in, w_out), (mix_in, mix_out))
+        )
+    ]
+    for copy in copies:
+        copy.start()
+    groups, blk = bias_out.shape
+    n = small_in.shape[0]
+    gh = groups * share // n
+    for g in range(groups):
+        total = 0.0
+        for part in range(g * share, (g + 1) * share):
+            row = 2 + part % gh
+            total = total + small_in[part // gh, row:row + 1, 0:blk]
+        bias_out[g:g + 1, :] = total * mix_scale
+    mine = small_in[lax.axis_index("sp")] * norm_scale
+    gain_out[...] = mine[0:1]
+    shift_out[...] = mine[1:2]
+    for copy in copies:
+        copy.wait()
 
 
 def local(cotangent, unit_pre, gate_pre, out_weight, mix_weight, mix_bias, norm_gain, norm_shift):
@@ -381,10 +426,11 @@
         V((8, ch), f32), V((m, 8, ch), f32), V((n, 8, ch), f32),
         V((m, rows, blk), bf16), V((m, rows, blk), bf16), V((n, m, rows, blk), bf16),
         V((hm, ch, dm), bf16), V((hm, ch, dm), bf16), V((hm, ch, dm), bf16), V((hm, ch, dm), bf16),
-        dma((2, n)), dma((2, n)),
+        dma((4, n)), dma((4, n)),
         dma((hm,)), dma((hm,)), dma((hm,)), dma((hm,)),
         dma((n,)), dma((n,)), dma((n,)), dma((n,)), dma((m,)), dma((m,)),
         dma((n,)), dma((n,)), dma((m,)), dma((m,)), dma((m,)), dma((m,)), dma((n,)), dma((n,)),
+        dma((n,)), dma((n,)),
         dma((hm,)), dma((hm,)), dma((hm,)), dma((hm,)), dma((2,)),
     ]
     unit_grad, gate_grad, w_grad, mix, small = pl.pallas_call(
@@ -407,12 +453,26 @@
         norm_gain[None], norm_shift[None],
     )
     share = group_dim // span
-    mix = jnp.sum(mix.reshape(groups, share, blk, blk), axis=1)
-    bias = jnp.sum(small[:, 2:2 + gh, :blk].reshape(groups, share, blk), axis=1) * mix_scale
-    mine = lax.dynamic_index_in_dim(small, lax.axis_index("sp"), 0, keepdims=False)
-    return (
-        unit_grad[None], gate_grad[None], w_grad, mix, bias, mine[0] * norm_scale, mine[1] * norm_scale,
-    )
+    unit_grad, gate_grad, w_grad, mix, bias, gain_grad, shift_grad = pl.pallas_call(
+        functools.partial(finish_kernel, share, mix_scale, norm_scale),
+        out_shape=(
+            jax.ShapeDtypeStruct((1, seq, ch), bf16),
+            jax.ShapeDtypeStruct((1, seq, ch), bf16),
+            jax.ShapeDtypeStruct((dm, ch), f32),
+            jax.ShapeDtypeStruct((n, m, rows, blk), f32),
+            jax.ShapeDtypeStruct((groups, blk), f32),
+            jax.ShapeDtypeStruct((1, ch), f32),
+            jax.ShapeDtypeStruct((1, ch), f32),
+        ),
+        in_specs=[vm] * 5,
+        out_specs=(hbm,) * 4 + (vm,) * 3,
+        scratch_shapes=[dma((4,))],
+    )(unit_grad, gate_grad, w_grad, mix, small)
+    if share == 1:
+        mix = mix.reshape(groups, blk, blk)
+    else:
+        mix = jnp.sum(mix.reshape(groups, share, blk, blk), axis=1)
+    return unit_grad, gate_grad, w_grad, mix, bias, gain_grad[0], shift_grad[0]
 
 
 def solution(mesh):

time: 76.2 us -> 70.2 us (0.921)
  local copies, waits for them, and re-layouts: 7.11 us -> 1.93 us
  other arithmetic: 2.7 us -> 0 us
  Pallas kernels: 65.3 us -> 67.2 us
    unnamed x14 -> x4, local copies, waits for them, and re-layouts: 5.95 us -> 0.77 us
    pallas_call x0 -> x1, Pallas kernels: none -> 3.46 us  [local(): pl.pallas_call(functools.partial(finish_kernel, share, mix_scale, norm_sc...]
    mul x2 -> x0, other arithmetic: 2.7 us -> none  [the longest x1 1.39 us: local(): mine[1] * norm_scale]
    pallas_call x1, Pallas kernels: 65.3 us -> 63.7 us  [local(): pl.pallas_call(functools.partial(kernel, n, m, width, group_dim, norm_sca...]
where the time goes in v2:
time: 70.2 us; the launch traced here: 69.8 us
  Pallas kernels  67.2 us (96%)
  local copies, waits for them, and re-layouts  1.93 us (3%)
    pallas_call x1, Pallas kernels, local(): pl.pallas_call(functools.partial(kernel, n, m, width, group_dim, norm_sca...  63.7 us
    pallas_call x1, Pallas kernels, local(): pl.pallas_call(functools.partial(finish_kernel, share, mix_scale, norm_sc...  3.46 us

profile of v2, /device:TPU:0, one launch (start us, length us, event | category | flops | bytes accessed | tf_op | source)
XLA Modules:
  0.0 69.8 jit_solution(4612169562216601956)
XLA Ops:
  0.6 0.0 copy-start
  0.6 0.7 copy-done
  1.3 0.0 copy-start.1
  1.3 0.6 broadcast_in_dim.6.gain
  1.9 0.1 copy-done.1
  2.0 0.6 broadcast_in_dim.7.shift
  2.6 63.7 %shard_map.135 = (bf16[512,512]{1,0:T(8,128)(2,1)}, bf16[512,512]{1,0:T(8,128)(2,1)}, f32[256,512]{1,0:T(8,128)}, f32[4,8,32,128]{3,2,1,0:T(8,128)}, f32[4,8,512]{2,1,0:T(8,128)}) custom-call(bf16[128,2048]{1,0:T(8,128)(2,1)} %bitcast.6, bf16[512,512]{1,0:T(8,128)(2,1)} %bitcast.7, bf16[512,512]{1,0:T(8,128)(2,1)} %bitcast.8, bf16[256,512]{1,0:T(8,128)(2,1)} %w.1, ...), custom_call_target="tpu_custom_call" | custom-call | tf_op jit(solution)/shard_map/pallas_call | solution.py:436
  66.3 3.5 %shard_map.136 = (bf16[1,512,512]{2,1,0:T(8,128)(2,1)}, bf16[1,512,512]{2,1,0:T(8,128)(2,1)}, f32[256,512]{1,0:T(8,128)}, f32[4,8,32,128]{3,2,1,0:T(8,128)}, f32...) custom-call(bf16[512,512]{1,0:T(8,128)(2,1)} %get-tuple-element.19.unit_in, ...), custom_call_target="tpu_custom_call" | custom-call | tf_op jit(solution)/shard_map/pallas_call | solution.py:456
Async XLA Ops:
  0.6 0.7 copy-start
  1.3 0.7 copy-start.1
